TPU v7x, 32 devices: a whole 2x2x4 slice. The times are simulated.
32 devices in a mesh: kv: 8 (over z, y), tp: 4 (over x, core).
Axes of the slice: x: 2, y: 2, z: 4, core: 2. Of those that a mesh axis runs over, the one named last changes fastest.
Arguments:
- tokens: bfloat16 [256, 4096], P(None, ('kv', 'tp')), may hold values from -60 to 60
- past_state: float32 [256, 16, 128, 128], P('kv', 'tp'), may hold values from -4 to 4
- pre_gain: float32 [4096], replicated, may hold values from 0.1 to 1.9
- pre_gate: bfloat16 [4096, 11264], P(None, ('kv', 'tp')), may hold values from -0.09375 to 0.09375
- pre_up: bfloat16 [4096, 11264], P(None, ('kv', 'tp')), may hold values from -0.09375 to 0.09375
- pre_down: bfloat16 [11264, 4096], P(('kv', 'tp')), may hold values from -0.109375 to 0.109375
- mix_gain: float32 [4096], replicated, may hold values from 0.1 to 1.9
- query_weight: bfloat16 [4096, 2048], P('kv', 'tp'), may hold values from -0.09375 to 0.09375
- forget_weight: bfloat16 [4096, 2048], P('kv', 'tp'), may hold values from -0.09375 to 0.09375
- value_weight: bfloat16 [4096, 2048], P('kv', 'tp'), may hold values from -0.09375 to 0.09375
- output_gate_weight: bfloat16 [4096, 2048], P('kv', 'tp'), may hold values from -0.09375 to 0.09375
- forget_floor: float32 [2048], P('tp'), may hold values from 0.02 to 0.9
- head_gain: float32 [128], replicated, may hold values from 0.1 to 1.9
- proj_out: bfloat16 [2048, 4096], P('tp', 'kv'), may hold values from -0.125 to 0.125
- post_gain: float32 [4096], replicated, may hold values from 0.1 to 1.9
- post_gate: bfloat16 [4096, 11264], P(None, ('kv', 'tp')), may hold values from -0.09375 to 0.09375
- post_up: bfloat16 [4096, 11264], P(None, ('kv', 'tp')), may hold values from -0.09375 to 0.09375
- post_down: bfloat16 [11264, 4096], P(('kv', 'tp')), may hold values from -0.109375 to 0.109375
Outputs:
- result: bfloat16 [256, 4096], P(None, ('kv', 'tp'))
- new_state: float32 [256, 16, 128, 128], P('kv', 'tp')
All inputs are finite; a program needn't handle non-finite values.
Results may differ from a plain program's by a relative error of at most 0.014.
Values may be sent and summed in bfloat16 or wider, within the bound.
A program may use at most 128 MiB of HBM per device.

v0:
```python
import jax
import jax.numpy as jnp
from jax import lax
from jax.sharding import PartitionSpec as P

D = 4096
epsilon = 1e-06


def half_inputs(activations, gain, w_gate, w_up):
    piece_float = lax.all_gather(activations, ("kv", "tp"), axis=1, tiled=True).astype(jnp.float32)
    normed = (piece_float * gain).astype(jnp.bfloat16)
    gate_acc = jnp.dot(normed, w_gate, preferred_element_type=jnp.float32)
    up_acc = jnp.dot(normed, w_up, preferred_element_type=jnp.float32)
    squares = jnp.sum(piece_float * piece_float, axis=1)
    row_scale = lax.rsqrt(squares / D + epsilon)[:, None]
    return (jax.nn.silu(row_scale * gate_acc) * (row_scale * up_acc)).astype(jnp.bfloat16)


def down_sum(hidden, w_down):
    return lax.psum_scatter(
        jnp.dot(hidden, w_down, preferred_element_type=jnp.float32),
        ("kv", "tp"),
        scatter_dimension=1,
        tiled=True,
    )


def per_device(
    tokens,
    past_state,
    pre_gain,
    pre_gate,
    pre_up,
    pre_down,
    mix_gain,
    query_weight,
    forget_weight,
    value_weight,
    output_gate_weight,
    forget_floor,
    head_gain,
    proj_out,
    post_gain,
    post_gate,
    post_up,
    post_down,
):
    whole_rows = lax.all_gather(tokens, ("kv", "tp"), axis=1, tiled=True)
    whole_float = whole_rows.astype(jnp.float32)
    row_scale = lax.rsqrt(jnp.mean(whole_float * whole_float, axis=1, keepdims=True) + epsilon)
    normed = (whole_float * pre_gain).astype(jnp.bfloat16)
    gate_pre = row_scale * jnp.dot(normed, pre_gate, preferred_element_type=jnp.float32)
    up_pre = row_scale * jnp.dot(normed, pre_up, preferred_element_type=jnp.float32)
    hidden = (jax.nn.silu(gate_pre) * up_pre).astype(jnp.bfloat16)
    kv_sums = lax.psum_scatter(
        jnp.dot(hidden, pre_down, preferred_element_type=jnp.float32).astype(jnp.bfloat16),
        "kv",
        scatter_dimension=1,
        tiled=True,
    )
    block_sum = lax.psum(kv_sums, "tp").astype(jnp.float32)
    block_width = block_sum.shape[1]
    block_old = lax.dynamic_slice_in_dim(
        whole_rows, lax.axis_index("kv") * block_width, block_width, 1
    )
    block_rows = (block_old.astype(jnp.float32) + 0.5 * block_sum).astype(jnp.bfloat16)
    own_width = block_width // lax.axis_size("tp")
    after_first = lax.dynamic_slice_in_dim(
        block_rows, lax.axis_index("tp") * own_width, own_width, 1
    )
    block_width = block_rows.shape[1]
    block_float = block_rows.astype(jnp.float32)
    block_gain = lax.dynamic_slice_in_dim(
        mix_gain, lax.axis_index("kv") * block_width, block_width, 0
    )
    squares = lax.psum(jnp.sum(block_float * block_float, axis=1), "kv")
    normed = (block_float * block_gain).astype(jnp.bfloat16)
    own_rows = past_state.shape[0]
    weight_list = (query_weight, forget_weight, value_weight, output_gate_weight)
    projected = lax.psum_scatter(
        jnp.concatenate(
            [
                jnp.dot(normed, weight_part, preferred_element_type=jnp.float32)
                for weight_part in weight_list
            ],
            axis=1,
        ).astype(jnp.bfloat16),
        "kv",
        scatter_dimension=0,
        tiled=True,
    ).astype(jnp.float32)
    own_squares = lax.dynamic_slice_in_dim(squares, lax.axis_index("kv") * own_rows, own_rows, 0)
    projected = projected * lax.rsqrt(own_squares / D + epsilon)[:, None]
    pre_query, pre_forget, pre_value, pre_gate_out = jnp.split(projected, 4, axis=1)
    local_heads = past_state.shape[1]
    head_width = past_state.shape[2]
    head_shape = (own_rows, local_heads, head_width)
    floors = forget_floor.reshape(local_heads, head_width)
    forget_heads = pre_forget.reshape(head_shape)
    forget = floors + (1.0 - floors) * jax.nn.sigmoid(forget_heads)
    written = (1.0 - floors) * jax.nn.sigmoid(-forget_heads)
    query_act = jax.nn.silu(pre_query.reshape(head_shape))
    value_act = pre_value.reshape(head_shape)
    new_state = (
        forget[:, :, :, None] * past_state + written[:, :, :, None] * value_act[:, :, None, :]
    )
    readout = jnp.einsum("bhkv,bhk->bhv", new_state, query_act, precision=lax.Precision.HIGHEST)
    readout = (
        readout
        * lax.rsqrt(jnp.mean(readout * readout, axis=2, keepdims=True) + epsilon)
        * head_gain
    )
    mixed_in = (
        readout.reshape(own_rows, local_heads * head_width) * jax.nn.silu(pre_gate_out)
    ).astype(jnp.bfloat16)
    partials = jnp.dot(
        lax.all_gather(mixed_in, "kv", axis=0, tiled=True),
        proj_out,
        preferred_element_type=jnp.float32,
    ).astype(jnp.bfloat16)
    mixed_sum = lax.psum_scatter(partials, "tp", scatter_dimension=1, tiled=True).astype(
        jnp.float32
    )
    second = (after_first.astype(jnp.float32) + mixed_sum).astype(jnp.bfloat16)
    hidden_two = half_inputs(second, post_gain, post_gate, post_up)
    result = (second.astype(jnp.float32) + 0.5 * down_sum(hidden_two, post_down)).astype(
        jnp.bfloat16
    )
    return (result, new_state)


def solution(mesh):
    placed = (
        P(None, ("kv", "tp")),
        P("kv", "tp", None, None),
        P(),
        P(None, ("kv", "tp")),
        P(None, ("kv", "tp")),
        P(("kv", "tp"), None),
        P(),
        P("kv", "tp"),
        P("kv", "tp"),
        P("kv", "tp"),
        P("kv", "tp"),
        P("tp"),
        P(),
        P("tp", "kv"),
        P(),
        P(None, ("kv", "tp")),
        P(None, ("kv", "tp")),
        P(("kv", "tp"), None),
    )
    return jax.shard_map(
        per_device,
        mesh=mesh,
        in_specs=placed,
        out_specs=(P(None, ("kv", "tp")), P("kv", "tp", None, None)),
        check_vma=False,
    )
```

profile of v0, /device:TPU:0, one launch (start us, length us, event | category | flops | bytes accessed | tf_op | source)
XLA Modules:
  0.0 548.7 jit_solution(15226853268982632663)
XLA Ops:
  7.2 0.0 all-gather.3.cloned.1.call-start
  7.2 0.7 all-gather.3.cloned.1.call-update
  7.9 0.0 reduce-scatter.7.cloned.1.call-start
  8.0 58.6 %all-gather.3.cloned.1.call-done = bf16[256,4096]{1,0:T(8,128)(2,1)} async-done(((bf16[256,128]{1,0:T(8,128)(2,1)}), bf16[256,4096]{1,0:T(8,128)(2,1)}) %all-gather.3.cloned.1.call-update) | async-done | bytes 2097168 | tf_op jit(solution)/shard_map/all_gather | solution.py:49
  66.6 2.1 fusion
  68.7 3.4 fusion.12
  72.1 7.5 %convolution_convert_fusion = bf16[256,4096]{1,0:T(8,128)(2,1)} fusion(bf16[352,4096]{1,0:T(8,128)(2,1)S(1)} %copy-done, bf16[4096,352]{0,1:T(8,128)(2,1)} %param.22, bf16[256,4096]{1,0:T(8,128)(2,1)} %all-gather.3.cloned.1.call-done, f32[4096]{0:T(1024)S(1)} %copy-done.7, f32[256,352]{0,1:T(8,128)S(1)} %fusion.12, f32[256]{0:T(256)S(1)} %add_rsqrt_fusion.2), kind=kOutput, calls=%fused_computation.5 | convolution fusion | flops 1481220096 | bytes 10339328 | tf_op jit(solution)/shard_map/dot_general | solution.py:57
  79.6 0.0 all-reduce.2.cloned.1.call-start
  79.7 68.1 %reduce-scatter.7.cloned.1.call-done = bf16[256,512]{1,0:T(8,128)(2,1)} async-done(((bf16[256,4096]{1,0:T(8,128)(2,1)}), bf16[256,512]{1,0:T(8,128)(2,1)}) %reduce-scatter.7.cloned.1.call-update) | async-done | bytes 262160 | tf_op jit(solution)/shard_map/reduce_scatter | solution.py:56
  147.8 0.0 reduce-scatter.9.cloned.1.call-start
  147.8 0.8 dynamic_slice.14
  148.6 32.8 %all-reduce.2.cloned.1.call-done = bf16[256,512]{1,0:T(8,128)(2,1)} async-done(((bf16[256,512]{1,0:T(8,128)(2,1)}), bf16[256,512]{1,0:T(8,128)(2,1)}) %all-reduce.2.cloned.1.call-update) | async-done | bytes 262160 | tf_op jit(solution)/shard_map/psum | solution.py:62
  181.4 1.2 fusion.42
  182.6 1.3 convolution_convert_fusion.3
  183.9 1.3 convolution_convert_fusion.2
  185.3 1.3 convolution_convert_fusion.4
  186.6 1.3 convolution_convert_fusion.5
  188.0 1.1 pad_maximum_fusion
  189.1 0.0 reduce-scatter.13.cloned.1.call-start
  189.2 21.6 %psum.15 = f32[256]{0:T(256)S(1)} all-reduce(f32[256]{0:T(256)S(1)} %get-tuple-element.2), channel_id=1, replica_groups=mesh['kv'=8,'tp'=4] {'kv'}, use_global_device_ids=true, to_apply=%region_5.6 | all-reduce | flops 256 | bytes 2048 | tf_op jit(solution)/shard_map/psum | solution.py:77
  210.8 0.1 add_rsqrt_fusion.3
  210.8 42.6 %reduce-scatter.9.cloned.1.call-done = bf16[32,2048]{1,0:T(8,128)(2,1)} async-done(((bf16[256,2048]{1,0:T(8,128)(2,1)}), bf16[32,2048]{1,0:T(8,128)(2,1)}) %reduce-scatter.9.cloned.1.call-update) | async-done | bytes 131088 | tf_op jit(solution)/shard_map/reduce_scatter | solution.py:81
  253.5 1.0 convert_multiply_fusion.6
  254.5 0.7 fusion.64
  255.1 0.6 reshape.74
  255.8 0.9 divide_multiply_fusion
  256.7 0.6 div.65
  257.3 0.9 mul.203
  258.2 1.5 div.63
  259.6 0.9 multiply_add_fusion.1
  260.5 8.2 %multiply_add_fusion = f32[32,4,128,128]{3,2,1,0:T(8,128)S(1)} fusion(f32[32,4,128,128]{3,2,1,0:T(8,128)} %param.19, f32[32,4,128]{2,1,0:T(4,128)S(1)} %mul.203, f32[32,4,128]{2,1,0:T(4,128)S(1)} %bitcast.39, f32[32,4,128]{2,1,0:T(4,128)S(1)} %bitcast.38), kind=kLoop, calls=%fused_computation | loop fusion | flops 6291456 | bytes 16973824 | tf_op jit(solution)/shard_map/add | solution.py:106
  268.8 7.2 %fusion.65 = f32[32,4,1,128]{3,2,1,0:T(1,128)S(1)} fusion(f32[32,4,128,128]{3,2,1,0:T(8,128)S(1)} %multiply_add_fusion, f32[32,4,128,1]{2,3,1,0:T(1,128)S(1)} %bitcast.37), kind=kOutput, calls=%fused_computation.68 | convolution fusion | flops 25165824 | bytes 8519680 | tf_op jit(solution)/shard_map/bhkv,bhk->bhv/dot_general | solution.py:108
  276.0 0.1 multiply_reduce_fusion
  276.1 0.1 multiply_multiply_fusion
  276.3 30.8 %all_gather.10 = bf16[256,512]{1,0:T(8,128)(2,1)S(1)} all-gather(bf16[32,512]{1,0:T(8,128)(2,1)S(1)} %fusion.61), channel_id=1, replica_groups=mesh['kv'=8,'tp'=4] {'kv'}, dimensions={0}, use_global_device_ids=true | all-gather | bytes 294912 | tf_op jit(solution)/shard_map/all_gather | solution.py:118
  307.1 0.3 convolution_convert_fusion.1
  307.4 0.8 copy.22
  308.3 0.0 all-gather.5.cloned.1.call-start
  308.3 19.2 %reduce-scatter.13.cloned.1.call-done = bf16[128,256]{1,0:T(8,128)(2,1)} async-done(((bf16[512,256]{1,0:T(8,128)(2,1)}), bf16[128,256]{1,0:T(8,128)(2,1)}) %reduce-scatter.13.cloned.1.call-update) | async-done | bytes 65552
  327.5 0.9 copy.23
  328.5 0.7 add_convert_fusion.2
  329.1 0.3 reduce-scatter.11.cloned.1.call-start
  329.4 54.4 %all-gather.5.cloned.1.call-done = bf16[256,4096]{1,0:T(8,128)(2,1)} async-done(((bf16[256,128]{1,0:T(8,128)(2,1)}), bf16[256,4096]{1,0:T(8,128)(2,1)}) %all-gather.5.cloned.1.call-update) | async-done | bytes 2097168 | tf_op jit(solution)/shard_map/all_gather | solution.py:11
  383.8 2.1 fusion.2
  385.9 3.4 fusion.18
  389.3 8.9 %fusion.37 = f32[256,4096]{1,0:T(8,128)} fusion(bf16[352,4096]{1,0:T(8,128)(2,1)} %param.35, bf16[4096,352]{0,1:T(8,128)(2,1)} %param.34, bf16[256,4096]{1,0:T(8,128)(2,1)} %all-gather.5.cloned.1.call-done, f32[4096]{0:T(1024)S(1)} %copy-done.4, f32[256,352]{0,1:T(8,128)S(1)} %fusion.18, f32[256]{0:T(256)S(1)} %add_rsqrt_fusion.1), kind=kOutput, calls=%fused_computation.27 | convolution fusion | flops 1480171520 | bytes 12436480 | tf_op jit(solution)/shard_map/dot_general | solution.py:22
  398.3 142.1 %reduce-scatter.11.cloned.1.call-done = f32[256,128]{1,0:T(8,128)} async-done(((f32[256,4096]{1,0:T(8,128)}), f32[256,128]{1,0:T(8,128)}) %reduce-scatter.11.cloned.1.call-update) | async-done | bytes 131088 | tf_op jit(solution)/shard_map/reduce_scatter | solution.py:21
  540.3 1.6 add_convert_fusion.1
  (29 shorter events, 0.2 us)
Async XLA Ops:
  7.2 65.0 %copy-start = (bf16[352,4096]{1,0:T(8,128)(2,1)S(1)}, bf16[352,4096]{1,0:T(8,128)(2,1)}, u32[]{:S(2)}) copy-start(bf16[352,4096]{1,0:T(8,128)(2,1)} %param.23) | copy-start | bytes 8650756
  7.2 59.4 %all-gather.3.cloned.1.call-start = ((), (), s32[]{:S(2)}) async-start(), calls=%async_computation.4 | async-start | bytes 2162688 | tf_op jit(solution)/shard_map/all_gather | solution.py:49
  7.9 139.8 %reduce-scatter.7.cloned.1.call-start = ((), (), s32[]{:S(2)}) async-start(), calls=%async_computation.5 | async-start | bytes 2359296 | tf_op jit(solution)/shard_map/reduce_scatter | solution.py:56
  68.7 3.5 copy-start.7
  79.6 101.7 %all-reduce.2.cloned.1.call-start = ((), (), s32[]{:S(2)}) async-start(), calls=%async_computation.6 | async-start | bytes 524288 | tf_op jit(solution)/shard_map/psum | solution.py:62
  147.8 105.7 %reduce-scatter.9.cloned.1.call-start = ((), (), s32[]{:S(2)}) async-start(), calls=%async_computation.7 | async-start | bytes 1179648 | tf_op jit(solution)/shard_map/reduce_scatter | solution.py:81
  185.3 3.9 copy-start.5
  189.1 138.4 %reduce-scatter.13.cloned.1.call-start = ((), (), s32[]{:S(2)}) async-start(), calls=%async_computation.10 | async-start | bytes 327680
  268.8 7.2 %copy-start.1 = (f32[32,4,128,128]{3,2,1,0:T(8,128)}, f32[32,4,128,128]{3,2,1,0:T(8,128)S(1)}, u32[]{:S(2)}) copy-start(f32[32,4,128,128]{3,2,1,0:T(8,128)S(1)} %multiply_add_fusion) | copy-start | bytes 25165828
  268.8 7.3 %copy-start.6 = (f32[128]{0:T(128)S(1)}, f32[128]{0:T(128)}, u32[]{:S(2)}) copy-start(f32[128]{0:T(128)} %param.30) | copy-start | bytes 1540
  268.8 38.3 %copy-start.3 = (bf16[512,512]{1,0:T(8,128)(2,1)S(1)}, bf16[512,512]{1,0:T(8,128)(2,1)}, u32[]{:S(2)}) copy-start(bf16[512,512]{1,0:T(8,128)(2,1)} %param.31) | copy-start | bytes 1572868
  276.0 109.9 %copy-start.4 = (f32[4096]{0:T(1024)S(1)}, f32[4096]{0:T(1024)}, u32[]{:S(2)}) copy-start(f32[4096]{0:T(1024)} %param.32) | copy-start | bytes 49156
  308.3 75.5 %all-gather.5.cloned.1.call-start = ((), (), s32[]{:S(2)}) async-start(), calls=%async_computation.8 | async-start | bytes 2162688 | tf_op jit(solution)/shard_map/all_gather | solution.py:11
  329.1 211.2 %reduce-scatter.11.cloned.1.call-start = ((), (), s32[]{:S(2)}) async-start(), calls=%async_computation.9 | async-start | bytes 4325376 | tf_op jit(solution)/shard_map/reduce_scatter | solution.py:21
  398.2 142.1 %copy-start.2 = (bf16[256,128]{1,0:T(8,128)(2,1)S(1)}, bf16[256,128]{1,0:T(8,128)(2,1)}, u32[]{:S(2)}) copy-start(bf16[256,128]{1,0:T(8,128)(2,1)} %add_convert_fusion.2) | copy-start | bytes 196612
Sparse Core Ops, SparseCore 0:
  10.8 55.6 all-gather.2
  79.7 67.9 reduce-scatter.6
  150.1 31.2 all-reduce.1
  189.2 64.1 reduce-scatter.8
  308.4 19.0 reduce-scatter.12
  330.8 52.9 all-gather.4
  398.4 141.8 reduce-scatter.10
where the time goes:
time: 550 us; the launch traced here: 549 us
  waiting for transfers between devices  418 us (76%)
  blocking collectives  52.4 us (10%)
  matrix products  36.1 us (7%)
  other arithmetic  20.7 us (4%)
  between operations  14.4 us (3%)
  local copies, waits for them, and re-layouts  6.21 us (1%)
    reduce_scatter x1, waiting for transfers between devices, down_sum(): lax.psum_scatter(jnp.dot(hidden, w_down, preferred_element_type=jnp.float...  142 us
    reduce_scatter x1, waiting for transfers between devices, per_device(): lax.psum_scatter(jnp.dot(hidden, pre_down, preferred_element_type=jnp.flo...  68.1 us
    all_gather x1, waiting for transfers between devices, per_device(): whole_rows = lax.all_gather(tokens, ('kv', 'tp'), axis=1, tiled=True)  58.6 us
    all_gather x1, waiting for transfers between devices, half_inputs(): lax.all_gather(activations, ('kv', 'tp'), axis=1, tiled=True)  54.4 us
    reduce_scatter x1, waiting for transfers between devices, per_device(): lax.psum_scatter(jnp.concatenate([jnp.dot(normed, weight_part, preferred_...  42.6 us
    psum x1, waiting for transfers between devices, per_device(): block_sum = lax.psum(kv_sums, 'tp').astype(jnp.float32)  32.8 us
    all_gather x1, blocking collectives, per_device(): lax.all_gather(mixed_in, 'kv', axis=0, tiled=True)  30.8 us
    psum x1, blocking collectives, per_device(): squares = lax.psum(jnp.sum(block_float * block_float, axis=1), 'kv')  21.6 us
  transfers between devices with their start and end apart: 7, of which 7 were waited for; matrix products, arithmetic and copies ran while one was open for 0% of the time, Pallas kernels for 0%

commit v1 on v0

--- a/solution.py
+++ b/solution.py
@@ -46,7 +46,8 @@
     post_up,
     post_down,
 ):
-    whole_rows = lax.all_gather(tokens, ("kv", "tp"), axis=1, tiled=True)
+    known = lax.all_gather(tokens, axis_name=("kv", "tp"))
+    whole_rows = jnp.concatenate(known, 1)
     whole_float = whole_rows.astype(jnp.float32)
     row_scale = lax.rsqrt(jnp.mean(whole_float * whole_float, axis=1, keepdims=True) + epsilon)
     normed = (whole_float * pre_gain).astype(jnp.bfloat16)

time: 550 us -> 554 us (level)
  local copies, waits for them, and re-layouts: 6.21 us -> 12.9 us
  transfers between devices with their start and end apart: 7 -> 7, of which waited for: 7 -> 7; matrix products, arithmetic and copies ran while one was open for 0% -> 1% of each run, Pallas kernels for 0% -> 0%
where the time goes in v1:
time: 554 us; the launch traced here: 553 us
  waiting for transfers between devices  418 us (75%)
  blocking collectives  52.5 us (9%)
  matrix products  33 us (6%)
  other arithmetic  22.2 us (4%)
  between operations  14.4 us (3%)
  local copies, waits for them, and re-layouts  12.9 us (2%)
    reduce_scatter x1, waiting for transfers between devices, down_sum(): lax.psum_scatter(jnp.dot(hidden, w_down, preferred_element_type=jnp.float...  142 us
    reduce_scatter x1, waiting for transfers between devices, per_device(): lax.psum_scatter(jnp.dot(hidden, pre_down, preferred_element_type=jnp.flo...  67.9 us
    all_gather x1, waiting for transfers between devices, per_device(): known = lax.all_gather(tokens, axis_name=('kv', 'tp'))  61.8 us
    all_gather x1, waiting for transfers between devices, half_inputs(): lax.all_gather(activations, ('kv', 'tp'), axis=1, tiled=True)  54.4 us
    reduce_scatter x1, waiting for transfers between devices, per_device(): lax.psum_scatter(jnp.concatenate([jnp.dot(normed, weight_part, preferred_...  42.6 us
    all_gather x1, blocking collectives, per_device(): lax.all_gather(mixed_in, 'kv', axis=0, tiled=True)  30.9 us
    psum x1, waiting for transfers between devices, per_device(): block_sum = lax.psum(kv_sums, 'tp').astype(jnp.float32)  28.9 us
    psum x1, blocking collectives, per_device(): squares = lax.psum(jnp.sum(block_float * block_float, axis=1), 'kv')  21.6 us
  transfers between devices with their start and end apart: 7, of which 7 were waited for; matrix products, arithmetic and copies ran while one was open for 1% of the time, Pallas kernels for 0%

profile of v1, /device:TPU:0, one launch (start us, length us, event | category | flops | bytes accessed | tf_op | source)
XLA Modules:
  0.0 553.1 jit_solution(11359648333969376564)
XLA Ops:
  7.2 0.7 all-gather.6.cloned.1.call-update
  8.0 61.8 %all-gather.6.cloned.1.call-done = bf16[8192,128]{1,0:T(8,128)(2,1)} async-done(((bf16[256,128]{1,0:T(8,128)(2,1)}), bf16[8192,128]{1,0:T(8,128)(2,1)}) %all-gather.6.cloned.1.call-update) | async-done | bytes 2097168 | tf_op jit(solution)/shard_map/all_gather | solution.py:49
  69.8 3.5 multiply_reduce_fusion
  73.3 1.4 copy.21
  74.7 1.3 copy-done.2
  76.0 1.3 fusion.14
  77.4 7.5 %convolution_convert_fusion = bf16[256,4096]{1,0:T(8,128)(2,1)} fusion(bf16[352,4096]{1,0:T(8,128)(2,1)S(1)} %copy-done, bf16[4096,352]{0,1:T(8,128)(2,1)} %param.22, f32[4096]{0:T(1024)S(1)} %copy-done.11, f32[256,352]{0,1:T(8,128)S(1)} %fusion.14, f32[256]{0:T(256)S(1)} %add_rsqrt_fusion.2, bf16[32,8,32,128]{3,2,1,0:T(8,128)(2,1)} %bitcast.49), kind=kOutput, calls=%fused_computation.3 | convolution fusion | flops 1481220096 | bytes 10339328 | tf_op jit(solution)/shard_map/dot_general | solution.py:58
  84.9 0.0 all-reduce.2.cloned.1.call-start
  84.9 67.9 %reduce-scatter.7.cloned.1.call-done = bf16[256,512]{1,0:T(8,128)(2,1)} async-done(((bf16[256,4096]{1,0:T(8,128)(2,1)}), bf16[256,512]{1,0:T(8,128)(2,1)}) %reduce-scatter.7.cloned.1.call-update) | async-done | bytes 262160 | tf_op jit(solution)/shard_map/reduce_scatter | solution.py:57
  152.9 0.8 dynamic_slice.14
  153.6 3.9 copy.38
  157.6 28.9 %all-reduce.2.cloned.1.call-done = bf16[256,512]{1,0:T(8,128)(2,1)} async-done(((bf16[256,512]{1,0:T(8,128)(2,1)}), bf16[256,512]{1,0:T(8,128)(2,1)}) %all-reduce.2.cloned.1.call-update) | async-done | bytes 262160 | tf_op jit(solution)/shard_map/psum | solution.py:63
  186.5 1.3 fusion.28
  187.8 1.3 convolution_convert_fusion.3
  189.1 1.3 convolution_convert_fusion.2
  190.5 1.4 convolution_convert_fusion.4
  191.9 0.3 convolution_convert_fusion.5
  192.2 1.1 pad_maximum_fusion
  193.3 0.0 reduce-scatter.13.cloned.1.call-start
  193.4 21.6 %psum.15 = f32[256]{0:T(256)S(1)} all-reduce(f32[256]{0:T(256)S(1)} %get-tuple-element.2), channel_id=1, replica_groups=mesh['kv'=8,'tp'=4] {'kv'}, use_global_device_ids=true, to_apply=%region_5.6 | all-reduce | flops 256 | bytes 2048 | tf_op jit(solution)/shard_map/psum | solution.py:78
  215.0 0.1 add_rsqrt_fusion.3
  215.1 42.6 %reduce-scatter.9.cloned.1.call-done = bf16[32,2048]{1,0:T(8,128)(2,1)} async-done(((bf16[256,2048]{1,0:T(8,128)(2,1)}), bf16[32,2048]{1,0:T(8,128)(2,1)}) %reduce-scatter.9.cloned.1.call-update) | async-done | bytes 131088 | tf_op jit(solution)/shard_map/reduce_scatter | solution.py:82
  257.7 1.0 convert_multiply_fusion.4
  258.7 0.7 fusion.50
  259.4 0.7 reshape.82
  260.0 0.9 divide_multiply_fusion
  260.9 0.7 div.65
  261.6 0.9 mul.204
  262.4 1.5 div.63
  263.9 0.9 multiply_add_fusion.1
  264.8 8.2 %multiply_add_fusion = f32[32,4,128,128]{3,2,1,0:T(8,128)S(1)} fusion(f32[32,4,128,128]{3,2,1,0:T(8,128)} %param.19, f32[32,4,128]{2,1,0:T(4,128)S(1)} %mul.204, f32[32,4,128]{2,1,0:T(4,128)S(1)} %bitcast.59, f32[32,4,128]{2,1,0:T(4,128)S(1)} %bitcast.58), kind=kLoop, calls=%fused_computation | loop fusion | flops 6291456 | bytes 16973824 | tf_op jit(solution)/shard_map/add | solution.py:107
  273.1 7.2 %fusion.51 = f32[32,4,1,128]{3,2,1,0:T(1,128)S(1)} fusion(f32[32,4,128,128]{3,2,1,0:T(8,128)S(1)} %multiply_add_fusion, f32[32,4,128,1]{2,3,1,0:T(1,128)S(1)} %bitcast.57), kind=kOutput, calls=%fused_computation.67 | convolution fusion | flops 25165824 | bytes 8519680 | tf_op jit(solution)/shard_map/bhkv,bhk->bhv/dot_general | solution.py:109
  280.3 0.1 multiply_reduce_fusion.1
  280.4 0.1 multiply_multiply_fusion
  280.6 30.9 %all_gather.14 = bf16[256,512]{1,0:T(8,128)(2,1)S(1)} all-gather(bf16[32,512]{1,0:T(8,128)(2,1)S(1)} %fusion.47), channel_id=1, replica_groups=mesh['kv'=8,'tp'=4] {'kv'}, dimensions={0}, use_global_device_ids=true | all-gather | bytes 294912 | tf_op jit(solution)/shard_map/all_gather | solution.py:119
  311.5 0.3 convolution_convert_fusion.1
  311.8 0.8 copy.24
  312.6 0.0 all-gather.4.cloned.1.call-start
  312.7 18.8 %reduce-scatter.13.cloned.1.call-done = bf16[128,256]{1,0:T(8,128)(2,1)} async-done(((bf16[512,256]{1,0:T(8,128)(2,1)}), bf16[128,256]{1,0:T(8,128)(2,1)}) %reduce-scatter.13.cloned.1.call-update) | async-done | bytes 65552
  331.5 0.9 copy.25
  332.4 0.7 add_convert_fusion.2
  333.1 0.3 reduce-scatter.11.cloned.1.call-start
  333.4 54.4 %all-gather.4.cloned.1.call-done = bf16[256,4096]{1,0:T(8,128)(2,1)} async-done(((bf16[256,128]{1,0:T(8,128)(2,1)}), bf16[256,4096]{1,0:T(8,128)(2,1)}) %all-gather.4.cloned.1.call-update) | async-done | bytes 2097168 | tf_op jit(solution)/shard_map/all_gather | solution.py:11
  387.8 2.1 fusion
  389.9 3.4 fusion.8
  393.3 9.0 %fusion.25 = f32[256,4096]{1,0:T(8,128)} fusion(bf16[352,4096]{1,0:T(8,128)(2,1)} %param.35, bf16[4096,352]{0,1:T(8,128)(2,1)} %param.34, bf16[256,4096]{1,0:T(8,128)(2,1)} %all-gather.4.cloned.1.call-done, f32[4096]{0:T(1024)S(1)} %copy-done.7, f32[256,352]{0,1:T(8,128)S(1)} %fusion.8, f32[256]{0:T(256)S(1)} %add_rsqrt_fusion.1), kind=kOutput, calls=%fused_computation.26 | convolution fusion | flops 1480171520 | bytes 12436480 | tf_op jit(solution)/shard_map/dot_general | solution.py:22
  402.3 142.4 %reduce-scatter.11.cloned.1.call-done = f32[256,128]{1,0:T(8,128)} async-done(((f32[256,4096]{1,0:T(8,128)}), f32[256,128]{1,0:T(8,128)}) %reduce-scatter.11.cloned.1.call-update) | async-done | bytes 131088 | tf_op jit(solution)/shard_map/reduce_scatter | solution.py:21
  544.7 1.6 add_convert_fusion.1
  (39 shorter events, 0.3 us)
Async XLA Ops:
  7.2 70.2 %copy-start = (bf16[352,4096]{1,0:T(8,128)(2,1)S(1)}, bf16[352,4096]{1,0:T(8,128)(2,1)}, u32[]{:S(2)}) copy-start(bf16[352,4096]{1,0:T(8,128)(2,1)} %param.23) | copy-start | bytes 8650756
  7.2 62.6 %all-gather.6.cloned.1.call-start = ((), (), s32[]{:S(2)}) async-start(), calls=%async_computation.9 | async-start | bytes 2162688 | tf_op jit(solution)/shard_map/all_gather | solution.py:49
  7.9 144.9 %reduce-scatter.7.cloned.1.call-start = ((), (), s32[]{:S(2)}) async-start(), calls=%async_computation.4 | async-start | bytes 2359296 | tf_op jit(solution)/shard_map/reduce_scatter | solution.py:57
  69.8 3.5 copy-start.3
  69.8 6.2 %copy-start.10 = (bf16[4096,352]{0,1:T(8,128)(2,1)S(1)}, bf16[4096,352]{0,1:T(8,128)(2,1)}, u32[]{:S(2)}) copy-start(bf16[4096,352]{0,1:T(8,128)(2,1)} %param.21) | copy-start | bytes 8650756
  69.8 6.2 %copy-start.11 = (f32[4096]{0:T(1024)S(1)}, f32[4096]{0:T(1024)}, u32[]{:S(2)}) copy-start(f32[4096]{0:T(1024)} %param.20) | copy-start | bytes 49156
  74.7 1.3 copy-start.2
  84.9 101.6 %all-reduce.2.cloned.1.call-start = ((), (), s32[]{:S(2)}) async-start(), calls=%async_computation.5 | async-start | bytes 524288 | tf_op jit(solution)/shard_map/psum | solution.py:63
  152.8 104.9 %reduce-scatter.9.cloned.1.call-start = ((), (), s32[]{:S(2)}) async-start(), calls=%async_computation.6 | async-start | bytes 1179648 | tf_op jit(solution)/shard_map/reduce_scatter | solution.py:82
  186.5 5.4 copy-start.5
  190.5 2.9 copy-start.8
  193.3 138.1 %reduce-scatter.13.cloned.1.call-start = ((), (), s32[]{:S(2)}) async-start(), calls=%async_computation.10 | async-start | bytes 327680
  273.0 7.2 %copy-start.1 = (f32[32,4,128,128]{3,2,1,0:T(8,128)}, f32[32,4,128,128]{3,2,1,0:T(8,128)S(1)}, u32[]{:S(2)}) copy-start(f32[32,4,128,128]{3,2,1,0:T(8,128)S(1)} %multiply_add_fusion) | copy-start | bytes 25165828
  273.0 7.3 %copy-start.9 = (f32[128]{0:T(128)S(1)}, f32[128]{0:T(128)}, u32[]{:S(2)}) copy-start(f32[128]{0:T(128)} %param.30) | copy-start | bytes 1540
  273.1 38.4 %copy-start.6 = (bf16[512,512]{1,0:T(8,128)(2,1)S(1)}, bf16[512,512]{1,0:T(8,128)(2,1)}, u32[]{:S(2)}) copy-start(bf16[512,512]{1,0:T(8,128)(2,1)} %param.31) | copy-start | bytes 1572868
  280.3 109.6 %copy-start.7 = (f32[4096]{0:T(1024)S(1)}, f32[4096]{0:T(1024)}, u32[]{:S(2)}) copy-start(f32[4096]{0:T(1024)} %param.32) | copy-start | bytes 49156
  312.6 75.1 %all-gather.4.cloned.1.call-start = ((), (), s32[]{:S(2)}) async-start(), calls=%async_computation.7 | async-start | bytes 2162688 | tf_op jit(solution)/shard_map/all_gather | solution.py:11
  333.1 211.6 %reduce-scatter.11.cloned.1.call-start = ((), (), s32[]{:S(2)}) async-start(), calls=%async_computation.8 | async-start | bytes 4325376 | tf_op jit(solution)/shard_map/reduce_scatter | solution.py:21
  402.2 142.4 %copy-start.4 = (bf16[256,128]{1,0:T(8,128)(2,1)S(1)}, bf16[256,128]{1,0:T(8,128)(2,1)}, u32[]{:S(2)}) copy-start(bf16[256,128]{1,0:T(8,128)(2,1)} %add_convert_fusion.2) | copy-start | bytes 196612
Sparse Core Ops, SparseCore 0:
  10.8 58.9 all-gather.5
  85.0 67.7 reduce-scatter.6
  155.1 31.3 all-reduce.1
  193.4 64.2 reduce-scatter.8
  312.8 18.6 reduce-scatter.12
  334.7 52.9 all-gather.3
  402.4 142.2 reduce-scatter.10
